TPU v7x, 32 devices: a whole 2x2x4 slice. The times are simulated.
32 devices in a mesh: fs: 8 (over z, y), tp: 4 (over x, core).
Axes of the slice: x: 2, y: 2, z: 4, core: 2. Of those that a mesh axis runs over, the one named last changes fastest.
Arguments:
- weights_in: float32 [2, 2048, 5632], P(None, 'fs', 'tp'), may hold values from -6 to 6
- weights_mix: float32 [2048, 2048], P('fs', 'tp'), may hold values from -6 to 6
- momentum_in: float32 [2, 2048, 5632], P(None, 'fs', 'tp'), may hold values from -5 to 5
- momentum_mix: float32 [2048, 2048], P('fs', 'tp'), may hold values from -5 to 5
- grads_in: float32 [2, 2048, 5632], P(None, 'fs', 'tp'), may hold values from -5 to 5
- grads_mix: float32 [2048, 2048], P('fs', 'tp'), may hold values from -5 to 5
Outputs:
- momentum_in_next: float32 [2, 2048, 5632], P(None, 'fs', 'tp')
- momentum_mix_next: float32 [2048, 2048], P('fs', 'tp')
- weights_in_next: float32 [2, 2048, 5632], P(None, 'fs', 'tp')
- weights_mix_next: float32 [2048, 2048], P('fs', 'tp')
- update_in: float32 [2, 2048, 5632], P(None, 'fs', 'tp')
- update_mix: float32 [2048, 2048], P('fs', 'tp')
All inputs are finite; a program needn't handle non-finite values.
Results may differ from a plain program's by a relative error of at most 0.0003.
Values sent between devices are 32-bit elements; how exact they have to be, the bound alone decides.
A program may use at most 128 MiB of HBM per device.

v0:
```python
import math
import jax
import jax.numpy as jnp
from jax import lax
from jax.sharding import PartitionSpec as P

D = 2048
FF = 5632
ITERS = 3
A_COEF = 3.4445
B_COEF = -4.775
C_COEF = 2.0315
MOMENTUM_DECAY = 0.95
STEP_RATE = 0.02
HIGH = lax.Precision.HIGHEST


def row_squares(shard):
    return jnp.sum(jnp.square(shard), axis=(1, 2))


def scale_from(summed):
    return (0.5 * lax.rsqrt(jnp.maximum(summed / D, 1.0)))[:, None, None]


def local(weights_in, weights_mix, momentum_in, momentum_mix, grads_in, grads_mix):
    moment_in = MOMENTUM_DECAY * momentum_in + grads_in
    moment_mix = MOMENTUM_DECAY * momentum_mix + grads_mix
    local_in = moment_in
    local_mix = moment_mix[None]
    squares = jnp.concatenate([row_squares(local_in), row_squares(local_mix)])
    scaling = scale_from(lax.psum(squares, ("fs", "tp")))
    for iteration in range(ITERS):
        cols_in, cols_mix = (
            lax.all_gather(local_in, "fs", axis=1, tiled=True),
            lax.all_gather(local_mix, "fs", axis=1, tiled=True),
        )
        partial_value = jnp.concatenate(
            [
                jnp.einsum("krc,ksc->krs", local_in, cols_in, precision=HIGH),
                jnp.einsum("krc,ksc->krs", local_mix, cols_mix, precision=HIGH),
            ]
        )
        gram_block = lax.psum_scatter(partial_value, "tp", scatter_dimension=2, tiled=True)
        gram_rows = lax.all_gather(gram_block, "tp", axis=2, tiled=True)
        factor = scaling if iteration == 0 else jnp.ones_like(scaling)
        gram_cols = lax.all_gather(gram_block, "fs", axis=1, tiled=True)
        square = jnp.einsum("krs,ksc->krc", gram_rows, gram_cols, precision=HIGH)
        poly_mat = factor**2 * B_COEF * gram_block + factor**4 * C_COEF * square
        poly_rows = lax.all_gather(poly_mat, "tp", axis=2, tiled=True)
        local_in = factor[:2] * (
            A_COEF * local_in + jnp.einsum("krs,ksc->krc", poly_rows[:2], cols_in, precision=HIGH)
        )
        local_mix = factor[2:] * (
            A_COEF * local_mix + jnp.einsum("krs,ksc->krc", poly_rows[2:], cols_mix, precision=HIGH)
        )
    step_in = local_in * math.sqrt(max(D, FF))
    step_mix = local_mix[0] * math.sqrt(D)
    return (
        moment_in,
        moment_mix,
        weights_in - STEP_RATE * step_in,
        weights_mix - STEP_RATE * step_mix,
        step_in,
        step_mix,
    )


def solution(mesh):
    in_specs = (
        P(None, "fs", "tp"),
        P("fs", "tp"),
        P(None, "fs", "tp"),
        P("fs", "tp"),
        P(None, "fs", "tp"),
        P("fs", "tp"),
    )
    out_specs = (
        P(None, "fs", "tp"),
        P("fs", "tp"),
        P(None, "fs", "tp"),
        P("fs", "tp"),
        P(None, "fs", "tp"),
        P("fs", "tp"),
    )
    return jax.shard_map(local, mesh=mesh, in_specs=in_specs, out_specs=out_specs, check_vma=False)
```

profile of v0, /device:TPU:0, one launch (start us, length us, event | category | flops | bytes accessed | tf_op | source)
XLA Modules:
  0.0 2754.7 jit_solution(12206210918786785973)
XLA Ops:
  7.2 0.0 all-gather.43.cloned.1.call-start
  7.2 2.7 multiply_reduce_fusion.1
  9.9 0.0 all-gather.43.cloned.1.call-update
  9.9 0.0 all-gather.19.cloned.1.call-start
  10.0 4.7 multiply_reduce_fusion
  14.7 0.0 all-gather.19.cloned.1.call-update
  14.7 0.0 reduce-scatter.4.cloned.1.call-start
  14.7 71.5 %all-gather.43.cloned.1.call-done = f32[2048,512]{1,0:T(8,128)} async-done(((f32[256,512]{1,0:T(8,128)}), f32[2048,512]{1,0:T(8,128)}) %all-gather.43.cloned.1.call-update) | async-done | bytes 4194320 | tf_op jit(solution)/shard_map/all_gather | solution.py:36
  86.2 7.1 convolution_bitcast_fusion.2
  93.4 434.6 %all-gather.19.cloned.1.call-done = f32[2,2048,1408]{2,1,0:T(8,128)} async-done(((f32[2,256,1408]{2,1,0:T(8,128)}), f32[2,2048,1408]{2,1,0:T(8,128)}) %all-gather.19.cloned.1.call-update) | async-done | bytes 23068688 | tf_op jit(solution)/shard_map/all_gather | solution.py:35
  528.0 24.5 fusion.8
  552.5 3.1 pad_maximum_fusion
  555.6 0.0 all-gather.21.cloned.1.call-start
  555.7 58.0 %reduce-scatter.4.cloned.1.call-done = f32[3,256,512]{2,1,0:T(8,128)} async-done(((f32[3,256,2048]{2,1,0:T(8,128)}), f32[3,256,512]{2,1,0:T(8,128)}) %reduce-scatter.4.cloned.1.call-update) | async-done | bytes 1572880 | tf_op jit(solution)/shard_map/reduce_scatter | solution.py:44
  613.7 0.0 all-gather.23.cloned.1.call-start
  613.7 0.5 all-gather.23.cloned.1.call-update
  614.3 0.0 all-gather.25.cloned.1.call-start
  614.3 0.7 pad_maximum_fusion.3
  615.0 40.5 %psum.7 = f32[3]{0:T(128)S(1)} all-reduce(f32[3]{0:T(128)S(1)} %pad_maximum_fusion.3), channel_id=1, replica_groups=mesh['fs'=8,'tp'=4] {'fs','tp'}, use_global_device_ids=true, to_apply=%region_2.0 | all-reduce | flops 3 | bytes 24 | tf_op jit(solution)/shard_map/psum | solution.py:32
  655.6 6.8 all-gather.21.cloned.1.call-done
  662.3 178.2 %all-gather.23.cloned.1.call-done = f32[3,2048,512]{2,1,0:T(8,128)} async-done(((f32[3,256,512]{2,1,0:T(8,128)}), f32[3,2048,512]{2,1,0:T(8,128)}) %all-gather.23.cloned.1.call-update) | async-done | bytes 12582928 | tf_op jit(solution)/shard_map/all_gather | solution.py:47
  840.5 17.5 multiply_add_fusion.3
  858.0 0.0 all-gather.45.cloned.1.call-start
  858.1 0.6 slice.28
  858.7 44.1 %all-gather.25.cloned.1.call-done = f32[3,256,2048]{2,1,0:T(8,128)} async-done(((f32[3,256,512]{2,1,0:T(8,128)}), f32[3,256,2048]{2,1,0:T(8,128)}) %all-gather.25.cloned.1.call-update) | async-done | bytes 6291472 | tf_op jit(solution)/shard_map/all_gather | solution.py:50
  902.7 8.0 fusion.5
  910.7 0.6 all-gather.27.cloned.1.call-start
  911.3 27.5 fusion
  938.8 0.2 reduce-scatter.6.cloned.1.call-start
  939.0 44.6 %all-gather.45.cloned.1.call-done = f32[2048,512]{1,0:T(8,128)} async-done(((f32[256,512]{1,0:T(8,128)}), f32[2048,512]{1,0:T(8,128)}) %all-gather.45.cloned.1.call-update) | async-done | bytes 4194320 | tf_op jit(solution)/shard_map/all_gather | solution.py:36
  983.7 7.1 convolution_bitcast_fusion.1
  990.8 434.6 %all-gather.27.cloned.1.call-done = f32[2,2048,1408]{2,1,0:T(8,128)} async-done(((f32[2,256,1408]{2,1,0:T(8,128)}), f32[2,2048,1408]{2,1,0:T(8,128)}) %all-gather.27.cloned.1.call-update) | async-done | bytes 23068688 | tf_op jit(solution)/shard_map/all_gather | solution.py:35
  1425.4 24.5 fusion.9
  1449.9 3.1 pad_maximum_fusion.1
  1453.1 0.0 all-gather.29.cloned.1.call-start
  1453.1 58.0 %reduce-scatter.6.cloned.1.call-done = f32[3,256,512]{2,1,0:T(8,128)} async-done(((f32[3,256,2048]{2,1,0:T(8,128)}), f32[3,256,512]{2,1,0:T(8,128)}) %reduce-scatter.6.cloned.1.call-update) | async-done | bytes 1572880 | tf_op jit(solution)/shard_map/reduce_scatter | solution.py:44
  1511.1 0.0 all-gather.31.cloned.1.call-start
  1511.2 0.7 all-gather.31.cloned.1.call-update
  1511.9 0.3 all-gather.33.cloned.1.call-start
  1512.1 46.8 %all-gather.29.cloned.1.call-done = f32[3,256,2048]{2,1,0:T(8,128)} async-done(((f32[3,256,512]{2,1,0:T(8,128)}), f32[3,256,2048]{2,1,0:T(8,128)}) %all-gather.29.cloned.1.call-update) | async-done | bytes 6291472 | tf_op jit(solution)/shard_map/all_gather | solution.py:45
  1558.9 178.3 %all-gather.31.cloned.1.call-done = f32[3,2048,512]{2,1,0:T(8,128)} async-done(((f32[3,256,512]{2,1,0:T(8,128)}), f32[3,2048,512]{2,1,0:T(8,128)}) %all-gather.31.cloned.1.call-update) | async-done | bytes 12582928 | tf_op jit(solution)/shard_map/all_gather | solution.py:47
  1737.2 17.5 multiply_add_fusion.2
  1754.8 0.0 all-gather.47.cloned.1.call-start
  1754.8 44.6 %all-gather.33.cloned.1.call-done = f32[3,256,2048]{2,1,0:T(8,128)} async-done(((f32[3,256,512]{2,1,0:T(8,128)}), f32[3,256,2048]{2,1,0:T(8,128)}) %all-gather.33.cloned.1.call-update) | async-done | bytes 6291472 | tf_op jit(solution)/shard_map/all_gather | solution.py:50
  1799.5 7.3 fusion.6
  1806.8 0.3 all-gather.35.cloned.1.call-start
  1807.1 27.4 convolution_add_fusion.1
  1834.5 0.5 reduce-scatter.8.cloned.1.call-start
  1835.0 44.7 %all-gather.47.cloned.1.call-done = f32[2048,512]{1,0:T(8,128)} async-done(((f32[256,512]{1,0:T(8,128)}), f32[2048,512]{1,0:T(8,128)}) %all-gather.47.cloned.1.call-update) | async-done | bytes 4194320 | tf_op jit(solution)/shard_map/all_gather | solution.py:36
  1879.7 7.1 convolution_bitcast_fusion
  1886.9 434.4 %all-gather.35.cloned.1.call-done = f32[2,2048,1408]{2,1,0:T(8,128)} async-done(((f32[2,256,1408]{2,1,0:T(8,128)}), f32[2,2048,1408]{2,1,0:T(8,128)}) %all-gather.35.cloned.1.call-update) | async-done | bytes 23068688 | tf_op jit(solution)/shard_map/all_gather | solution.py:35
  2321.3 24.5 fusion.10
  2345.9 3.1 pad_maximum_fusion.2
  2349.0 0.0 all-gather.37.cloned.1.call-start
  2349.1 58.0 %reduce-scatter.8.cloned.1.call-done = f32[3,256,512]{2,1,0:T(8,128)} async-done(((f32[3,256,2048]{2,1,0:T(8,128)}), f32[3,256,512]{2,1,0:T(8,128)}) %reduce-scatter.8.cloned.1.call-update) | async-done | bytes 1572880 | tf_op jit(solution)/shard_map/reduce_scatter | solution.py:44
  2407.0 0.0 all-gather.39.cloned.1.call-start
  2407.1 0.5 all-gather.39.cloned.1.call-update
  2407.6 0.2 all-gather.41.cloned.1.call-start
  2407.9 47.0 %all-gather.37.cloned.1.call-done = f32[3,256,2048]{2,1,0:T(8,128)} async-done(((f32[3,256,512]{2,1,0:T(8,128)}), f32[3,256,2048]{2,1,0:T(8,128)}) %all-gather.37.cloned.1.call-update) | async-done | bytes 6291472 | tf_op jit(solution)/shard_map/all_gather | solution.py:45
  2454.8 178.2 %all-gather.39.cloned.1.call-done = f32[3,2048,512]{2,1,0:T(8,128)} async-done(((f32[3,256,512]{2,1,0:T(8,128)}), f32[3,2048,512]{2,1,0:T(8,128)}) %all-gather.39.cloned.1.call-update) | async-done | bytes 12582928 | tf_op jit(solution)/shard_map/all_gather | solution.py:47
  2633.0 17.5 multiply_add_fusion.1
  2650.5 44.7 %all-gather.41.cloned.1.call-done = f32[3,256,2048]{2,1,0:T(8,128)} async-done(((f32[3,256,512]{2,1,0:T(8,128)}), f32[3,256,2048]{2,1,0:T(8,128)}) %all-gather.41.cloned.1.call-update) | async-done | bytes 6291472 | tf_op jit(solution)/shard_map/all_gather | solution.py:50
  2695.2 46.1 %broadcast_multiply_fusion = (f32[2,256,1408]{2,1,0:T(8,128)}, f32[2,256,1408]{2,1,0:T(8,128)}) fusion(f32[2,256,1408]{2,1,0:T(8,128)} %param.6, f32[3,256,2048]{2,1,0:T(8,128)} %all-gather.41.cloned.1.call-done, f32[2,2048,1408]{2,1,0:T(8,128)} %all-gather.35.cloned.1.call-done, f32[2,256,1408]{2,1,0:T(8,128)S(1)} %copy-done.2), kind=kOutput, calls=%fused_computation.22 | convolution fusion | flops 17720344576 | bytes 40894464 | tf_op jit(solution)/shard_map/krs,ksc->krc/dot_general | solution.py:52
  2741.3 6.3 broadcast_multiply_fusion.1
  (37 shorter events, 0.3 us)
Async XLA Ops:
  7.2 79.1 %all-gather.43.cloned.1.call-start = ((), (), s32[]{:S(2)}) async-start(), calls=%async_computation.18 | async-start | bytes 4718592 | tf_op jit(solution)/shard_map/all_gather | solution.py:36
  9.9 76.3 %copy-start.9 = (f32[256,512]{1,0:T(8,128)S(1)}, f32[256,512]{1,0:T(8,128)}, u32[]{:S(2)}) copy-start(f32[256,512]{1,0:T(8,128)} %get-tuple-element.11) | copy-start | bytes 1572868
  9.9 518.0 %all-gather.19.cloned.1.call-start = ((), (), s32[]{:S(2)}) async-start(), calls=%async_computation.3 | async-start | bytes 25952256 | tf_op jit(solution)/shard_map/all_gather | solution.py:35
  14.7 513.3 %copy-start = (f32[2,256,1408]{2,1,0:T(8,128)S(1)}, f32[2,256,1408]{2,1,0:T(8,128)}, u32[]{:S(2)}) copy-start(f32[2,256,1408]{2,1,0:T(8,128)} %get-tuple-element.9) | copy-start | bytes 8650756
  14.7 599.0 %reduce-scatter.4.cloned.1.call-start = ((), (), s32[]{:S(2)}) async-start(), calls=%async_computation.4 | async-start | bytes 7864320 | tf_op jit(solution)/shard_map/reduce_scatter | solution.py:44
  528.0 24.6 copy-start.6
  555.6 106.7 %all-gather.21.cloned.1.call-start = ((), (), s32[]{:S(2)}) async-start(), calls=%async_computation.5 | async-start | bytes 7864320 | tf_op jit(solution)/shard_map/all_gather | solution.py:45
  613.7 226.8 %all-gather.23.cloned.1.call-start = ((), (), s32[]{:S(2)}) async-start(), calls=%async_computation.6 | async-start | bytes 14155776 | tf_op jit(solution)/shard_map/all_gather | solution.py:47
  614.3 288.5 %all-gather.25.cloned.1.call-start = ((), (), s32[]{:S(2)}) async-start(), calls=%async_computation.7 | async-start | bytes 7864320 | tf_op jit(solution)/shard_map/all_gather | solution.py:50
  858.0 125.6 %all-gather.45.cloned.1.call-start = ((), (), s32[]{:S(2)}) async-start(), calls=%async_computation.19 | async-start | bytes 4718592 | tf_op jit(solution)/shard_map/all_gather | solution.py:36
  910.7 514.7 %all-gather.27.cloned.1.call-start = ((), (), s32[]{:S(2)}) async-start(), calls=%async_computation.8 | async-start | bytes 25952256 | tf_op jit(solution)/shard_map/all_gather | solution.py:35
  911.3 72.4 %copy-start.5 = (f32[256,512]{1,0:T(8,128)S(1)}, f32[256,512]{1,0:T(8,128)}, u32[]{:S(2)}) copy-start(f32[256,512]{1,0:T(8,128)} %fusion.5) | copy-start | bytes 1572868
  938.8 486.6 %copy-start.1 = (f32[2,256,1408]{2,1,0:T(8,128)S(1)}, f32[2,256,1408]{2,1,0:T(8,128)}, u32[]{:S(2)}) copy-start(f32[2,256,1408]{2,1,0:T(8,128)} %fusion) | copy-start | bytes 8650756
  938.8 572.3 %reduce-scatter.6.cloned.1.call-start = ((), (), s32[]{:S(2)}) async-start(), calls=%async_computation.9 | async-start | bytes 7864320 | tf_op jit(solution)/shard_map/reduce_scatter | solution.py:44
  1425.4 24.6 copy-start.7
  1453.1 105.8 %all-gather.29.cloned.1.call-start = ((), (), s32[]{:S(2)}) async-start(), calls=%async_computation.10 | async-start | bytes 7864320 | tf_op jit(solution)/shard_map/all_gather | solution.py:45
  1511.1 226.1 %all-gather.31.cloned.1.call-start = ((), (), s32[]{:S(2)}) async-start(), calls=%async_computation.11 | async-start | bytes 14155776 | tf_op jit(solution)/shard_map/all_gather | solution.py:47
  1511.9 287.6 %all-gather.33.cloned.1.call-start = ((), (), s32[]{:S(2)}) async-start(), calls=%async_computation.12 | async-start | bytes 7864320 | tf_op jit(solution)/shard_map/all_gather | solution.py:50
  1754.8 125.0 %all-gather.47.cloned.1.call-start = ((), (), s32[]{:S(2)}) async-start(), calls=%async_computation.20 | async-start | bytes 4718592 | tf_op jit(solution)/shard_map/all_gather | solution.py:36
  1806.8 73.0 %copy-start.4 = (f32[256,512]{1,0:T(8,128)S(1)}, f32[256,512]{1,0:T(8,128)}, u32[]{:S(2)}) copy-start(f32[256,512]{1,0:T(8,128)} %fusion.6) | copy-start | bytes 1572868
  1806.8 514.5 %all-gather.35.cloned.1.call-start = ((), (), s32[]{:S(2)}) async-start(), calls=%async_computation.13 | async-start | bytes 25952256 | tf_op jit(solution)/shard_map/all_gather | solution.py:35
  1834.5 486.8 %copy-start.2 = (f32[2,256,1408]{2,1,0:T(8,128)S(1)}, f32[2,256,1408]{2,1,0:T(8,128)}, u32[]{:S(2)}) copy-start(f32[2,256,1408]{2,1,0:T(8,128)} %convolution_add_fusion.1) | copy-start | bytes 8650756
  1834.5 572.5 %reduce-scatter.8.cloned.1.call-start = ((), (), s32[]{:S(2)}) async-start(), calls=%async_computation.14 | async-start | bytes 7864320 | tf_op jit(solution)/shard_map/reduce_scatter | solution.py:44
  2321.3 24.6 copy-start.8
  2349.0 105.8 %all-gather.37.cloned.1.call-start = ((), (), s32[]{:S(2)}) async-start(), calls=%async_computation.15 | async-start | bytes 7864320 | tf_op jit(solution)/shard_map/all_gather | solution.py:45
  2407.0 225.9 %all-gather.39.cloned.1.call-start = ((), (), s32[]{:S(2)}) async-start(), calls=%async_computation.16 | async-start | bytes 14155776 | tf_op jit(solution)/shard_map/all_gather | solution.py:47
  2407.6 287.6 %all-gather.41.cloned.1.call-start = ((), (), s32[]{:S(2)}) async-start(), calls=%async_computation.17 | async-start | bytes 7864320 | tf_op jit(solution)/shard_map/all_gather | solution.py:50
  2695.2 46.1 %copy-start.3 = (f32[2048,512]{1,0:T(8,128)S(1)}, f32[2048,512]{1,0:T(8,128)}, u32[]{:S(2)}) copy-start(f32[2048,512]{1,0:T(8,128)} %all-gather.47.cloned.1.call-done) | copy-start | bytes 12582916
  2695.2 46.1 %copy-start.10 = (f32[256,512]{1,0:T(8,128)S(1)}, f32[256,512]{1,0:T(8,128)}, u32[]{:S(2)}) copy-start(f32[256,512]{1,0:T(8,128)} %param.7) | copy-start | bytes 1572868
Sparse Core Ops, SparseCore 0:
  10.7 75.5 all-gather.42
  88.3 439.5 all-gather.18
  555.8 57.8 reduce-scatter.3
  615.1 47.2 all-gather.20
  664.4 176.0 all-gather.22
  858.2 44.5 all-gather.24
  910.8 72.7 all-gather.44
  985.8 439.5 all-gather.26
  1453.2 57.8 reduce-scatter.5
  1512.5 46.3 all-gather.28
  1561.1 176.0 all-gather.30
  1754.9 44.5 all-gather.32
  1806.9 72.7 all-gather.46
  1881.7 439.5 all-gather.34
  2349.1 57.8 reduce-scatter.7
  2408.4 46.3 all-gather.36
  2456.8 176.0 all-gather.38
  2650.7 44.5 all-gather.40
where the time goes:
time: 2760 us; the launch traced here: 2750 us
  waiting for transfers between devices  2410 us (87%)
  matrix products  270 us (10%)
  blocking collectives  40.5 us (1%)
    all_gather x3, waiting for transfers between devices, local(): lax.all_gather(local_in, 'fs', axis=1, tiled=True)  1300 us
    all_gather x3, waiting for transfers between devices, local(): gram_cols = lax.all_gather(gram_block, 'fs', axis=1, tiled=True)  535 us
    reduce_scatter x3, waiting for transfers between devices, local(): lax.psum_scatter(partial_value, 'tp', scatter_dimension=2, tiled=True)  174 us
    all_gather x3, waiting for transfers between devices, local(): lax.all_gather(local_mix, 'fs', axis=1, tiled=True)  161 us
    all_gather x3, waiting for transfers between devices, local(): poly_rows = lax.all_gather(poly_mat, 'tp', axis=2, tiled=True)  133 us
    dot_general x3, matrix products, local(): jnp.einsum('krs,ksc->krc', poly_rows[:2], cols_in, precision=HIGH)  101 us
    all_gather x3, waiting for transfers between devices, local(): gram_rows = lax.all_gather(gram_block, 'tp', axis=2, tiled=True)  100 us
    dot_general x3, matrix products, local(): jnp.einsum('krc,ksc->krs', local_in, cols_in, precision=HIGH)  73.6 us
  transfers between devices with their start and end apart: 18, of which 18 were waited for; matrix products, arithmetic and copies ran while one was open for 3% of the time, Pallas kernels for 0%

commit v1 on v0

--- a/solution.py
+++ b/solution.py
@@ -32,7 +32,9 @@
     scaling = scale_from(lax.psum(squares, ("fs", "tp")))
     for iteration in range(ITERS):
         cols_in, cols_mix = (
-            lax.all_gather(local_in, "fs", axis=1, tiled=True),
+            jnp.concatenate(
+                lax.all_to_all(jnp.stack([local_in] * lax.axis_size("fs")), "fs", 0, 0), axis=1
+            ),
             lax.all_gather(local_mix, "fs", axis=1, tiled=True),
         )
         partial_value = jnp.concatenate(

time: 2760 us -> 2980 us (1.080)
  waiting for transfers between devices: 2410 us -> 2550 us
  local copies, waits for them, and re-layouts: 0.63 us -> 58.7 us
    all_gather x3 -> x0, waiting for transfers between devices: 1300 us -> none  [local(): lax.all_gather(local_in, 'fs', axis=1, tiled=True)]
    all_gather x3, waiting for transfers between devices: 161 us -> 1310 us  [local(): lax.all_gather(local_mix, 'fs', axis=1, tiled=True)]
    all_to_all x0 -> x3, waiting for transfers between devices: none -> 293 us  [local(): lax.all_to_all(jnp.stack([local_in] * lax.axis_size('fs')), 'fs', 0, 0)]
    another operation x0 -> x3, local copies, waits for them, and re-layouts: none -> 31.4 us  [local(): jnp.stack([local_in] * lax.axis_size('fs'))]
  transfers between devices with their start and end apart: 18 -> 18, of which waited for: 18 -> 18; matrix products, arithmetic and copies ran while one was open for 3% -> 1% of each run, Pallas kernels for 0% -> 0%
where the time goes in v1:
time: 2980 us; the launch traced here: 2970 us
  waiting for transfers between devices  2550 us (86%)
  matrix products  267 us (9%)
  local copies, waits for them, and re-layouts  58.7 us (2%)
  blocking collectives  40.4 us (1%)
    all_gather x3, waiting for transfers between devices, local(): lax.all_gather(local_mix, 'fs', axis=1, tiled=True)  1310 us
    all_gather x3, waiting for transfers between devices, local(): gram_cols = lax.all_gather(gram_block, 'fs', axis=1, tiled=True)  535 us
    all_to_all x3, waiting for transfers between devices, local(): lax.all_to_all(jnp.stack([local_in] * lax.axis_size('fs')), 'fs', 0, 0)  293 us
    reduce_scatter x3, waiting for transfers between devices, local(): lax.psum_scatter(partial_value, 'tp', scatter_dimension=2, tiled=True)  169 us
    all_gather x3, waiting for transfers between devices, local(): poly_rows = lax.all_gather(poly_mat, 'tp', axis=2, tiled=True)  134 us
    all_gather x3, waiting for transfers between devices, local(): gram_rows = lax.all_gather(gram_block, 'tp', axis=2, tiled=True)  101 us
    dot_general x3, matrix products, local(): jnp.einsum('krs,ksc->krc', poly_rows[:2], cols_in, precision=HIGH)  101 us
    dot_general x3, matrix products, local(): jnp.einsum('krc,ksc->krs', local_in, cols_in, precision=HIGH)  71.3 us
  transfers between devices with their start and end apart: 18, of which 18 were waited for; matrix products, arithmetic and copies ran while one was open for 1% of the time, Pallas kernels for 0%

profile of v1, /device:TPU:0, one launch (start us, length us, event | category | flops | bytes accessed | tf_op | source)
XLA Modules:
  0.0 2970.1 jit_solution(11591520641135120827)
XLA Ops:
  7.2 3.2 multiply_reduce_fusion
  10.4 9.9 stack.6
  20.2 7.4 all-to-all-start
  27.7 2.5 multiply_reduce_fusion.1
  30.3 0.0 reduce-scatter.4.cloned.1.call-start
  30.3 441.2 %all-gather.34.cloned.1.call-done = f32[2048,512]{1,0:T(8,128)} async-done(((f32[256,512]{1,0:T(8,128)}), f32[2048,512]{1,0:T(8,128)}) %all-gather.34.cloned.1.call-update) | async-done | bytes 4194320 | tf_op jit(solution)/shard_map/all_gather | solution.py:38
  471.5 7.3 convolution_bitcast_fusion.2
  478.8 97.7 %all-to-all-done = f32[8,2,256,1408]{3,2,1,0:T(8,128)} async-done(((f32[8,2,256,1408]{3,2,1,0:T(8,128)}), f32[8,2,256,1408]{3,2,1,0:T(8,128)}, u32[]{:S(2)}, u32[]{:S(2)}) %all-to-all-start) | async-done | bytes 23068704 | tf_op jit(solution)/shard_map/all_to_all | solution.py:36
  576.5 9.0 copy.12
  585.6 22.5 fusion.8
  608.1 5.5 pad_maximum_fusion
  613.7 0.0 all-gather.16.cloned.1.call-start
  613.7 57.0 %reduce-scatter.4.cloned.1.call-done = f32[3,256,512]{2,1,0:T(8,128)} async-done(((f32[3,256,2048]{2,1,0:T(8,128)}), f32[3,256,512]{2,1,0:T(8,128)}) %reduce-scatter.4.cloned.1.call-update) | async-done | bytes 1572880 | tf_op jit(solution)/shard_map/reduce_scatter | solution.py:46
  670.8 0.5 all-gather.18.cloned.1.call-update
  671.3 0.0 all-gather.20.cloned.1.call-start
  671.4 0.7 pad_maximum_fusion.3
  672.1 40.4 %psum.7 = f32[3]{0:T(128)S(1)} all-reduce(f32[3]{0:T(128)S(1)} %pad_maximum_fusion.3), channel_id=1, replica_groups=mesh['fs'=8,'tp'=4] {'fs','tp'}, use_global_device_ids=true, to_apply=%region_2.0 | all-reduce | flops 3 | bytes 24 | tf_op jit(solution)/shard_map/psum | solution.py:32
  712.5 7.1 all-gather.16.cloned.1.call-done
  719.6 178.2 %all-gather.18.cloned.1.call-done = f32[3,2048,512]{2,1,0:T(8,128)} async-done(((f32[3,256,512]{2,1,0:T(8,128)}), f32[3,2048,512]{2,1,0:T(8,128)}) %all-gather.18.cloned.1.call-update) | async-done | bytes 12582928 | tf_op jit(solution)/shard_map/all_gather | solution.py:49
  897.7 17.5 multiply_add_fusion.3
  915.2 44.7 %all-gather.20.cloned.1.call-done = f32[3,256,2048]{2,1,0:T(8,128)} async-done(((f32[3,256,512]{2,1,0:T(8,128)}), f32[3,256,2048]{2,1,0:T(8,128)}) %all-gather.20.cloned.1.call-update) | async-done | bytes 6291472 | tf_op jit(solution)/shard_map/all_gather | solution.py:52
  959.9 27.8 fusion
  987.7 11.7 stack.7
  999.4 6.4 all-to-all-start.1
  1005.8 0.0 all-gather.36.cloned.1.call-start
  1005.8 0.6 slice.28
  1006.4 8.0 fusion.5
  1014.4 0.2 reduce-scatter.6.cloned.1.call-start
  1014.6 435.0 %all-gather.36.cloned.1.call-done = f32[2048,512]{1,0:T(8,128)} async-done(((f32[256,512]{1,0:T(8,128)}), f32[2048,512]{1,0:T(8,128)}) %all-gather.36.cloned.1.call-update) | async-done | bytes 4194320 | tf_op jit(solution)/shard_map/all_gather | solution.py:38
  1449.6 7.3 convolution_bitcast_fusion.1
  1456.9 97.8 %all-to-all-done.1 = f32[8,2,256,1408]{3,2,1,0:T(8,128)} async-done(((f32[8,2,256,1408]{3,2,1,0:T(8,128)}), f32[8,2,256,1408]{3,2,1,0:T(8,128)}, u32[]{:S(2)}, u32[]{:S(2)}) %all-to-all-start.1) | async-done | bytes 23068704 | tf_op jit(solution)/shard_map/all_to_all | solution.py:36
  1554.7 8.8 copy.13
  1563.5 24.4 fusion.9
  1587.9 4.8 pad_maximum_fusion.1
  1592.8 0.0 all-gather.22.cloned.1.call-start
  1592.8 56.1 %reduce-scatter.6.cloned.1.call-done = f32[3,256,512]{2,1,0:T(8,128)} async-done(((f32[3,256,2048]{2,1,0:T(8,128)}), f32[3,256,512]{2,1,0:T(8,128)}) %reduce-scatter.6.cloned.1.call-update) | async-done | bytes 1572880 | tf_op jit(solution)/shard_map/reduce_scatter | solution.py:46
  1649.0 0.7 all-gather.24.cloned.1.call-update
  1649.7 0.4 all-gather.26.cloned.1.call-start
  1650.1 46.7 %all-gather.22.cloned.1.call-done = f32[3,256,2048]{2,1,0:T(8,128)} async-done(((f32[3,256,512]{2,1,0:T(8,128)}), f32[3,256,2048]{2,1,0:T(8,128)}) %all-gather.22.cloned.1.call-update) | async-done | bytes 6291472 | tf_op jit(solution)/shard_map/all_gather | solution.py:47
  1696.9 178.3 %all-gather.24.cloned.1.call-done = f32[3,2048,512]{2,1,0:T(8,128)} async-done(((f32[3,256,512]{2,1,0:T(8,128)}), f32[3,2048,512]{2,1,0:T(8,128)}) %all-gather.24.cloned.1.call-update) | async-done | bytes 12582928 | tf_op jit(solution)/shard_map/all_gather | solution.py:49
  1875.2 16.1 multiply_add_fusion.2
  1891.3 44.7 %all-gather.26.cloned.1.call-done = f32[3,256,2048]{2,1,0:T(8,128)} async-done(((f32[3,256,512]{2,1,0:T(8,128)}), f32[3,256,2048]{2,1,0:T(8,128)}) %all-gather.26.cloned.1.call-update) | async-done | bytes 6291472 | tf_op jit(solution)/shard_map/all_gather | solution.py:52
  1936.0 26.9 convolution_add_fusion.1
  1962.9 9.9 stack.8
  1972.8 6.4 all-to-all-start.2
  1979.1 0.0 all-gather.38.cloned.1.call-start
  1979.2 7.3 fusion.6
  1986.5 0.0 reduce-scatter.8.cloned.1.call-start
  1986.6 436.4 %all-gather.38.cloned.1.call-done = f32[2048,512]{1,0:T(8,128)} async-done(((f32[256,512]{1,0:T(8,128)}), f32[2048,512]{1,0:T(8,128)}) %all-gather.38.cloned.1.call-update) | async-done | bytes 4194320 | tf_op jit(solution)/shard_map/all_gather | solution.py:38
  2423.0 7.3 convolution_bitcast_fusion
  2430.3 97.8 %all-to-all-done.2 = f32[8,2,256,1408]{3,2,1,0:T(8,128)} async-done(((f32[8,2,256,1408]{3,2,1,0:T(8,128)}), f32[8,2,256,1408]{3,2,1,0:T(8,128)}, u32[]{:S(2)}, u32[]{:S(2)}) %all-to-all-start.2) | async-done | bytes 23068704 | tf_op jit(solution)/shard_map/all_to_all | solution.py:36
  2528.1 8.8 copy.14
  2536.9 24.4 fusion.10
  2561.3 4.8 pad_maximum_fusion.2
  2566.1 0.0 all-gather.28.cloned.1.call-start
  2566.2 56.1 %reduce-scatter.8.cloned.1.call-done = f32[3,256,512]{2,1,0:T(8,128)} async-done(((f32[3,256,2048]{2,1,0:T(8,128)}), f32[3,256,512]{2,1,0:T(8,128)}) %reduce-scatter.8.cloned.1.call-update) | async-done | bytes 1572880 | tf_op jit(solution)/shard_map/reduce_scatter | solution.py:46
  2622.4 0.5 all-gather.30.cloned.1.call-update
  2622.9 0.0 all-gather.32.cloned.1.call-start
  2622.9 47.3 %all-gather.28.cloned.1.call-done = f32[3,256,2048]{2,1,0:T(8,128)} async-done(((f32[3,256,512]{2,1,0:T(8,128)}), f32[3,256,2048]{2,1,0:T(8,128)}) %all-gather.28.cloned.1.call-update) | async-done | bytes 6291472 | tf_op jit(solution)/shard_map/all_gather | solution.py:47
  2670.2 178.2 %all-gather.30.cloned.1.call-done = f32[3,2048,512]{2,1,0:T(8,128)} async-done(((f32[3,256,512]{2,1,0:T(8,128)}), f32[3,2048,512]{2,1,0:T(8,128)}) %all-gather.30.cloned.1.call-update) | async-done | bytes 12582928 | tf_op jit(solution)/shard_map/all_gather | solution.py:49
  2848.4 17.7 multiply_add_fusion.1
  2866.1 44.7 %all-gather.32.cloned.1.call-done = f32[3,256,2048]{2,1,0:T(8,128)} async-done(((f32[3,256,512]{2,1,0:T(8,128)}), f32[3,256,2048]{2,1,0:T(8,128)}) %all-gather.32.cloned.1.call-update) | async-done | bytes 6291472 | tf_op jit(solution)/shard_map/all_gather | solution.py:52
  2910.8 46.1 %broadcast_multiply_fusion = (f32[2,256,1408]{2,1,0:T(8,128)}, f32[2,256,1408]{2,1,0:T(8,128)}) fusion(f32[2,256,1408]{2,1,0:T(8,128)} %param.6, f32[3,256,2048]{2,1,0:T(8,128)} %all-gather.32.cloned.1.call-done, f32[2,2048,1408]{2,1,0:T(8,128)} %bitcast.64, f32[2,256,1408]{2,1,0:T(8,128)S(1)} %copy-done.5), kind=kOutput, calls=%fused_computation.22 | convolution fusion | flops 17720344576 | bytes 40894464 | tf_op jit(solution)/shard_map/krs,ksc->krc/dot_general | solution.py:54
  2957.0 6.3 broadcast_multiply_fusion.1
  (46 shorter events, 0.4 us)
Async XLA Ops:
  10.4 949.6 %copy-start.3 = (f32[2,256,1408]{2,1,0:T(8,128)}, f32[2,256,1408]{2,1,0:T(8,128)S(1)}, u32[]{:S(2)}) copy-start(f32[2,256,1408]{2,1,0:T(8,128)S(1)} %get-tuple-element.9) | copy-start | bytes 8650756
  20.2 7.5 copy-start.13
  20.2 556.3 %all-to-all-start = ((f32[8,2,256,1408]{3,2,1,0:T(8,128)}), f32[8,2,256,1408]{3,2,1,0:T(8,128)}, u32[]{:S(2)}, u32[]{:S(2)}) async-start(f32[8,2,256,1408]{3,2,1,0:T(8,128)} %stack.6), calls=%async_computation | async-start | bytes 46137344 | tf_op jit(solution)/shard_map/all_to_all | solution.py:36
  27.7 443.8 %all-gather.34.cloned.1.call-start = ((), (), s32[]{:S(2)}) async-start(), calls=%async_computation.18 | async-start | bytes 4718592 | tf_op jit(solution)/shard_map/all_gather | solution.py:38
  30.3 640.5 %reduce-scatter.4.cloned.1.call-start = ((), (), s32[]{:S(2)}) async-start(), calls=%async_computation.6 | async-start | bytes 7864320 | tf_op jit(solution)/shard_map/reduce_scatter | solution.py:46
  585.5 22.6 copy-start
  585.5 22.6 copy-start.10
  613.7 105.9 %all-gather.16.cloned.1.call-start = ((), (), s32[]{:S(2)}) async-start(), calls=%async_computation.7 | async-start | bytes 7864320 | tf_op jit(solution)/shard_map/all_gather | solution.py:47
  670.8 227.0 %all-gather.18.cloned.1.call-start = ((), (), s32[]{:S(2)}) async-start(), calls=%async_computation.8 | async-start | bytes 14155776 | tf_op jit(solution)/shard_map/all_gather | solution.py:49
  671.3 288.6 %all-gather.20.cloned.1.call-start = ((), (), s32[]{:S(2)}) async-start(), calls=%async_computation.9 | async-start | bytes 7864320 | tf_op jit(solution)/shard_map/all_gather | solution.py:52
  999.4 7.0 copy-start.11
  999.4 555.3 %all-to-all-start.1 = ((f32[8,2,256,1408]{3,2,1,0:T(8,128)}), f32[8,2,256,1408]{3,2,1,0:T(8,128)}, u32[]{:S(2)}, u32[]{:S(2)}) async-start(f32[8,2,256,1408]{3,2,1,0:T(8,128)} %stack.7), calls=%async_computation.2 | async-start | bytes 46137344 | tf_op jit(solution)/shard_map/all_to_all | solution.py:36
  1005.8 443.8 %all-gather.36.cloned.1.call-start = ((), (), s32[]{:S(2)}) async-start(), calls=%async_computation.19 | async-start | bytes 4718592 | tf_op jit(solution)/shard_map/all_gather | solution.py:38
  1014.4 634.5 %reduce-scatter.6.cloned.1.call-start = ((), (), s32[]{:S(2)}) async-start(), calls=%async_computation.10 | async-start | bytes 7864320 | tf_op jit(solution)/shard_map/reduce_scatter | solution.py:46
  1563.5 24.4 copy-start.2
  1592.8 104.1 %all-gather.22.cloned.1.call-start = ((), (), s32[]{:S(2)}) async-start(), calls=%async_computation.11 | async-start | bytes 7864320 | tf_op jit(solution)/shard_map/all_gather | solution.py:47
  1648.9 226.3 %copy-start.7 = (f32[3,256,512]{2,1,0:T(8,128)S(1)}, f32[3,256,512]{2,1,0:T(8,128)}, u32[]{:S(2)}) copy-start(f32[3,256,512]{2,1,0:T(8,128)} %reduce-scatter.6.cloned.1.call-done) | copy-start | bytes 4718596
  1648.9 226.3 %all-gather.24.cloned.1.call-start = ((), (), s32[]{:S(2)}) async-start(), calls=%async_computation.12 | async-start | bytes 14155776 | tf_op jit(solution)/shard_map/all_gather | solution.py:49
  1649.7 286.3 %all-gather.26.cloned.1.call-start = ((), (), s32[]{:S(2)}) async-start(), calls=%async_computation.13 | async-start | bytes 7864320 | tf_op jit(solution)/shard_map/all_gather | solution.py:52
  1962.9 9.9 copy-start.4
  1972.8 6.4 copy-start.9
  1972.8 555.3 %all-to-all-start.2 = ((f32[8,2,256,1408]{3,2,1,0:T(8,128)}), f32[8,2,256,1408]{3,2,1,0:T(8,128)}, u32[]{:S(2)}, u32[]{:S(2)}) async-start(f32[8,2,256,1408]{3,2,1,0:T(8,128)} %stack.8), calls=%async_computation.4 | async-start | bytes 46137344 | tf_op jit(solution)/shard_map/all_to_all | solution.py:36
  1979.1 443.8 %all-gather.38.cloned.1.call-start = ((), (), s32[]{:S(2)}) async-start(), calls=%async_computation.20 | async-start | bytes 4718592 | tf_op jit(solution)/shard_map/all_gather | solution.py:38
  1986.5 635.7 %reduce-scatter.8.cloned.1.call-start = ((), (), s32[]{:S(2)}) async-start(), calls=%async_computation.14 | async-start | bytes 7864320 | tf_op jit(solution)/shard_map/reduce_scatter | solution.py:46
  2536.9 24.4 copy-start.1
  2566.1 104.1 %all-gather.28.cloned.1.call-start = ((), (), s32[]{:S(2)}) async-start(), calls=%async_computation.15 | async-start | bytes 7864320 | tf_op jit(solution)/shard_map/all_gather | solution.py:47
  2622.3 226.1 %all-gather.30.cloned.1.call-start = ((), (), s32[]{:S(2)}) async-start(), calls=%async_computation.16 | async-start | bytes 14155776 | tf_op jit(solution)/shard_map/all_gather | solution.py:49
  2622.9 287.9 %copy-start.5 = (f32[2,256,1408]{2,1,0:T(8,128)S(1)}, f32[2,256,1408]{2,1,0:T(8,128)}, u32[]{:S(2)}) copy-start(f32[2,256,1408]{2,1,0:T(8,128)} %copy-done.4) | copy-start | bytes 8650756
  2622.9 287.9 %all-gather.32.cloned.1.call-start = ((), (), s32[]{:S(2)}) async-start(), calls=%async_computation.17 | async-start | bytes 7864320 | tf_op jit(solution)/shard_map/all_gather | solution.py:52
  2866.1 90.8 %copy-start.8 = (f32[256,512]{1,0:T(8,128)S(1)}, f32[256,512]{1,0:T(8,128)}, u32[]{:S(2)}) copy-start(f32[256,512]{1,0:T(8,128)} %fusion.6) | copy-start | bytes 1572868
  2910.8 46.1 %copy-start.6 = (f32[2048,512]{1,0:T(8,128)S(1)}, f32[2048,512]{1,0:T(8,128)}, u32[]{:S(2)}) copy-start(f32[2048,512]{1,0:T(8,128)} %all-gather.38.cloned.1.call-done) | copy-start | bytes 12582916
  2910.8 46.1 %copy-start.12 = (f32[256,512]{1,0:T(8,128)S(1)}, f32[256,512]{1,0:T(8,128)}, u32[]{:S(2)}) copy-start(f32[256,512]{1,0:T(8,128)} %param.7) | copy-start | bytes 1572868
Sparse Core Ops, SparseCore 0:
  31.2 440.2 all-gather.33
  613.8 56.8 reduce-scatter.3
  672.3 47.2 all-gather.15
  721.6 176.0 all-gather.17
  915.4 44.5 all-gather.19
  1014.5 435.0 all-gather.35
  1592.9 55.9 reduce-scatter.5
  1650.5 46.3 all-gather.21
  1699.1 176.0 all-gather.23
  1891.4 44.5 all-gather.25
  1986.7 436.2 all-gather.37
  2566.3 55.9 reduce-scatter.7
  2623.8 46.3 all-gather.27
  2672.3 176.0 all-gather.29
  2866.3 44.5 all-gather.31
